TPU v7x, 32 devices: a whole 2x2x4 slice. The times are simulated.
32 devices in a mesh: fs: 8 (over z, x), tp: 4 (over y, core).
Axes of the slice: x: 2, y: 2, z: 4, core: 2. Of those that a mesh axis runs over, the one named last changes fastest.
Arguments:
- prompt_rows: bfloat16 [512, 3072], P('tp'), may hold values from -6 to 6
- gate_first: float32 [3072, 8192], P('fs', 'tp'), may hold values from -0.109375 to 0.109375
- up_first: float32 [3072, 8192], P('fs', 'tp'), may hold values from -0.109375 to 0.109375
- down_first: float32 [8192, 3072], P('fs', 'tp'), may hold values from -0.0625 to 0.0625
- gate_second: float32 [3072, 8192], P('fs', 'tp'), may hold values from -0.109375 to 0.109375
- up_second: float32 [3072, 8192], P('fs', 'tp'), may hold values from -0.109375 to 0.109375
- down_second: float32 [8192, 3072], P('fs', 'tp'), may hold values from -0.0625 to 0.0625
- pre_gain_first: float32 [3072], replicated, may hold values from 0.1 to 1.9
- post_gain_first: float32 [3072], replicated, may hold values from 0.1 to 1.9
- pre_gain_second: float32 [3072], replicated, may hold values from 0.1 to 1.9
- post_gain_second: float32 [3072], replicated, may hold values from 0.1 to 1.9
Outputs:
- result_rows: bfloat16 [512, 3072], P('tp')
- gate_first_new: bfloat16 [3072, 8192], P(None, 'fs')
- up_first_new: bfloat16 [3072, 8192], P(None, 'fs')
- down_first_new: bfloat16 [8192, 3072], P('fs')
- gate_second_new: bfloat16 [3072, 8192], P(None, 'fs')
- up_second_new: bfloat16 [3072, 8192], P(None, 'fs')
- down_second_new: bfloat16 [8192, 3072], P('fs')
All inputs are finite; a program needn't handle non-finite values.
Results may differ from a plain program's by a relative error of at most 0.0071.
Values may be sent and summed in bfloat16 or wider, within the bound.
A program may use at most 192 MiB of HBM per device.

v0:
```python
import jax
import jax.numpy as jnp
from jax import lax
from jax.sharding import PartitionSpec as P

EPSILON = 1e-06


def half_step(rows, gate, up, down, post_gain):
    floats = rows.astype(jnp.float32)
    normed = (
        floats * lax.rsqrt(jnp.mean(floats * floats, axis=-1, keepdims=True) + EPSILON)
    ).astype(jnp.bfloat16)
    gate_pre = jnp.dot(normed, gate, preferred_element_type=jnp.float32)
    up_pre = jnp.dot(normed, up, preferred_element_type=jnp.float32)
    hidden = (jax.nn.silu(gate_pre) * up_pre).astype(jnp.bfloat16)
    partial_value = jnp.dot(hidden, down, preferred_element_type=jnp.float32)
    total = lax.psum(partial_value, "fs")
    scale = lax.rsqrt(jnp.mean(total * total, axis=-1, keepdims=True) + EPSILON)
    return (floats + 0.5 * total * scale * post_gain[None, :]).astype(jnp.bfloat16)


def per_device(
    prompt_rows,
    gate_first,
    up_first,
    down_first,
    gate_second,
    up_second,
    down_second,
    pre_gain_first,
    post_gain_first,
    pre_gain_second,
    post_gain_second,
):
    height = gate_first.shape[0]
    start = lax.axis_index("fs") * height
    gain_a = lax.dynamic_slice_in_dim(pre_gain_first, start, height, 0)[:, None]
    gain_b = lax.dynamic_slice_in_dim(pre_gain_second, start, height, 0)[:, None]
    wide = (
        lax.all_gather((gain_a * gate_first).astype(jnp.bfloat16), "tp", axis=1, tiled=True),
        lax.all_gather((gain_a * up_first).astype(jnp.bfloat16), "tp", axis=1, tiled=True),
        lax.all_gather(down_first.astype(jnp.bfloat16), "tp", axis=1, tiled=True),
        lax.all_gather((gain_b * gate_second).astype(jnp.bfloat16), "tp", axis=1, tiled=True),
        lax.all_gather((gain_b * up_second).astype(jnp.bfloat16), "tp", axis=1, tiled=True),
        lax.all_gather(down_second.astype(jnp.bfloat16), "tp", axis=1, tiled=True),
    )
    gate_a, up_a, gate_b, up_b = (
        lax.all_to_all(wide[0], "fs", split_axis=1, concat_axis=0, tiled=True),
        lax.all_to_all(wide[1], "fs", split_axis=1, concat_axis=0, tiled=True),
        lax.all_to_all(wide[3], "fs", split_axis=1, concat_axis=0, tiled=True),
        lax.all_to_all(wide[4], "fs", split_axis=1, concat_axis=0, tiled=True),
    )
    down_a = wide[2]
    down_b = wide[5]
    middle = half_step(prompt_rows, gate_a, up_a, down_a, post_gain_first)
    result = half_step(middle, gate_b, up_b, down_b, post_gain_second)
    return (result, gate_a, up_a, down_a, gate_b, up_b, down_b)


def solution(mesh):
    return jax.shard_map(
        per_device,
        mesh=mesh,
        in_specs=(
            P("tp", None),
            P("fs", "tp"),
            P("fs", "tp"),
            P("fs", "tp"),
            P("fs", "tp"),
            P("fs", "tp"),
            P("fs", "tp"),
            P(),
            P(),
            P(),
            P(),
        ),
        out_specs=(
            P("tp", None),
            P(None, "fs"),
            P(None, "fs"),
            P("fs", None),
            P(None, "fs"),
            P(None, "fs"),
            P("fs", None),
        ),
        check_vma=False,
    )
```

profile of v0, /device:TPU:0, one launch (start us, length us, event | category | flops | bytes accessed | tf_op | source)
XLA Modules:
  0.0 843.3 jit_solution(3647729259422297711)
XLA Ops:
  7.2 0.0 all-gather.7.cloned.1.call-start
  7.2 0.8 dynamic_slice.6
  8.0 5.5 multiply_convert_fusion.3
  13.5 0.0 all-gather.7.cloned.1.call-update
  13.5 0.0 all-gather.9.cloned.1.call-start
  13.6 0.7 all-gather.9.cloned.1.call-update
  14.3 48.5 %all-gather.7.cloned.1.call-done = bf16[384,8192]{1,0:T(8,128)(2,1)} async-done(((bf16[384,2048]{1,0:T(8,128)(2,1)}), bf16[384,8192]{1,0:T(8,128)(2,1)}) %all-gather.7.cloned.1.call-update) | async-done | bytes 6291472 | tf_op jit(solution)/shard_map/all_gather | solution.py:41
  62.7 6.5 copy.33
  69.2 5.8 all-to-all-start
  75.0 0.0 all-gather.13.cloned.1.call-start
  75.1 0.8 dynamic_slice.7
  75.8 0.0 copy-done.1
  75.8 4.5 multiply_convert_fusion.1
  80.4 0.0 all-gather.13.cloned.1.call-update
  80.4 30.9 %all-gather.9.cloned.1.call-done = bf16[384,8192]{1,0:T(8,128)(2,1)} async-done(((bf16[384,2048]{1,0:T(8,128)(2,1)}), bf16[384,8192]{1,0:T(8,128)(2,1)}) %all-gather.9.cloned.1.call-update) | async-done | bytes 6291472 | tf_op jit(solution)/shard_map/all_gather | solution.py:42
  111.3 6.5 copy.32
  117.8 95.9 %all-to-all-done = bf16[384,8,1024]{2,0,1:T(8,128)(2,1)} async-done(((bf16[384,8,1024]{2,0,1:T(8,128)(2,1)}), bf16[384,8,1024]{2,0,1:T(8,128)(2,1)}, u32[]{:S(2)}, u32[]{:S(2)}) %all-to-all-start) | async-done | bytes 6291488 | tf_op jit(solution)/shard_map/all_to_all | solution.py:49
  213.7 4.8 all-to-all-start.1
  218.4 0.0 all-gather.15.cloned.1.call-start
  218.5 0.5 all-gather.15.cloned.1.call-update
  219.0 0.0 all-gather.13.cloned.1.call-done
  219.0 6.5 copy.31
  225.5 130.6 %all-to-all-done.1 = bf16[384,8,1024]{2,0,1:T(8,128)(2,1)} async-done(((bf16[384,8,1024]{2,0,1:T(8,128)(2,1)}), bf16[384,8,1024]{2,0,1:T(8,128)(2,1)}, u32[]{:S(2)}, u32[]{:S(2)}) %all-to-all-start.1) | async-done | bytes 6291488 | tf_op jit(solution)/shard_map/all_to_all | solution.py:50
  356.1 4.8 all-to-all-start.2
  361.0 0.0 copy-start
  361.0 0.0 all-gather.11.cloned.1.call-start
  361.0 3.2 convert_element_type.47
  364.3 0.0 all-gather.11.cloned.1.call-update
  364.3 0.0 all-reduce.3.cloned.1.call-start
  364.3 0.0 copy-done
  364.4 0.2 fusion
  364.6 0.0 all-gather.15.cloned.1.call-done
  364.6 6.5 copy.30
  371.1 4.6 fusion.26
  375.7 35.5 %all-gather.11.cloned.1.call-done = bf16[1024,3072]{1,0:T(8,128)(2,1)} async-done(((bf16[1024,768]{1,0:T(8,128)(2,1)}), bf16[1024,3072]{1,0:T(8,128)(2,1)}) %all-gather.11.cloned.1.call-update) | async-done | bytes 6291472 | tf_op jit(solution)/shard_map/all_gather | solution.py:43
  411.2 7.7 fusion.9
  418.9 0.0 all-reduce.3.cloned.1.call-update
  418.9 100.4 %all-to-all-done.2 = bf16[384,8,1024]{2,0,1:T(8,128)(2,1)} async-done(((bf16[384,8,1024]{2,0,1:T(8,128)(2,1)}), bf16[384,8,1024]{2,0,1:T(8,128)(2,1)}, u32[]{:S(2)}, u32[]{:S(2)}) %all-to-all-start.2) | async-done | bytes 6291488 | tf_op jit(solution)/shard_map/all_to_all | solution.py:51
  519.3 4.8 all-to-all-start.3
  524.1 0.0 copy-start.2
  524.1 0.0 all-gather.17.cloned.1.call-start
  524.2 3.3 convert_element_type.54
  527.4 0.0 all-gather.17.cloned.1.call-update
  527.4 0.2 all-reduce.5.cloned.1.call-start
  527.7 130.8 %all-reduce.3.cloned.1.call-done = f32[128,3072]{1,0:T(8,128)} async-done(((f32[128,3072]{1,0:T(8,128)}), f32[128,3072]{1,0:T(8,128)}) %all-reduce.3.cloned.1.call-update) | async-done | bytes 1572880 | tf_op jit(solution)/shard_map/psum | solution.py:18
  658.5 1.6 multiply_reduce_fusion.1
  660.1 0.0 copy-done.2
  660.1 1.9 fusion.3
  662.0 4.2 fusion.22
  666.3 38.0 %all-gather.17.cloned.1.call-done = bf16[1024,3072]{1,0:T(8,128)(2,1)} async-done(((bf16[1024,768]{1,0:T(8,128)(2,1)}), bf16[1024,3072]{1,0:T(8,128)(2,1)}) %all-gather.17.cloned.1.call-update) | async-done | bytes 6291472 | tf_op jit(solution)/shard_map/all_gather | solution.py:46
  704.2 0.0 all-to-all-done.3
  704.2 7.7 fusion.8
  711.9 0.0 all-reduce.5.cloned.1.call-update
  712.0 89.4 %all-reduce.5.cloned.1.call-done = f32[128,3072]{1,0:T(8,128)} async-done(((f32[128,3072]{1,0:T(8,128)}), f32[128,3072]{1,0:T(8,128)}) %all-reduce.5.cloned.1.call-update) | async-done | bytes 1572880 | tf_op jit(solution)/shard_map/psum | solution.py:18
  801.4 1.6 multiply_reduce_fusion
  803.0 0.0 copy-done.3
  803.0 2.6 fusion.5
  805.6 6.4 copy.42
  812.0 6.3 copy.43
  818.3 2.7 copy.44
  821.0 6.4 copy.45
  827.4 6.3 copy.46
  833.8 0.0 slice-done.2
  833.8 2.7 copy.47
  (15 shorter events, 0.1 us)
Async XLA Ops:
  7.2 55.6 %all-gather.7.cloned.1.call-start = ((), (), s32[]{:S(2)}) async-start(), calls=%async_computation.4 | async-start | bytes 7864320 | tf_op jit(solution)/shard_map/all_gather | solution.py:41
  13.5 97.8 %all-gather.9.cloned.1.call-start = ((), (), s32[]{:S(2)}) async-start(), calls=%async_computation.5 | async-start | bytes 7864320 | tf_op jit(solution)/shard_map/all_gather | solution.py:42
  69.2 6.6 copy-start.1
  69.2 144.4 %all-to-all-start = ((bf16[384,8,1024]{2,0,1:T(8,128)(2,1)}), bf16[384,8,1024]{2,0,1:T(8,128)(2,1)}, u32[]{:S(2)}, u32[]{:S(2)}) async-start(bf16[384,8,1024]{2,0,1:T(8,128)(2,1)} %bitcast.40), calls=%async_computation | async-start | bytes 12582912 | tf_op jit(solution)/shard_map/all_to_all | solution.py:49
  75.0 144.0 %all-gather.13.cloned.1.call-start = ((), (), s32[]{:S(2)}) async-start(), calls=%async_computation.8 | async-start | bytes 7864320 | tf_op jit(solution)/shard_map/all_gather | solution.py:44
  213.7 142.5 %all-to-all-start.1 = ((bf16[384,8,1024]{2,0,1:T(8,128)(2,1)}), bf16[384,8,1024]{2,0,1:T(8,128)(2,1)}, u32[]{:S(2)}, u32[]{:S(2)}) async-start(bf16[384,8,1024]{2,0,1:T(8,128)(2,1)} %bitcast.41), calls=%async_computation.1 | async-start | bytes 12582912 | tf_op jit(solution)/shard_map/all_to_all | solution.py:50
  218.4 146.2 %all-gather.15.cloned.1.call-start = ((), (), s32[]{:S(2)}) async-start(), calls=%async_computation.9 | async-start | bytes 7864320 | tf_op jit(solution)/shard_map/all_gather | solution.py:45
  356.1 163.1 %all-to-all-start.2 = ((bf16[384,8,1024]{2,0,1:T(8,128)(2,1)}), bf16[384,8,1024]{2,0,1:T(8,128)(2,1)}, u32[]{:S(2)}, u32[]{:S(2)}) async-start(bf16[384,8,1024]{2,0,1:T(8,128)(2,1)} %bitcast.39), calls=%async_computation.2 | async-start | bytes 12582912 | tf_op jit(solution)/shard_map/all_to_all | solution.py:51
  361.0 3.4 copy-start
  361.0 50.2 %all-gather.11.cloned.1.call-start = ((), (), s32[]{:S(2)}) async-start(), calls=%async_computation.6 | async-start | bytes 7864320 | tf_op jit(solution)/shard_map/all_gather | solution.py:43
  364.3 294.2 %all-reduce.3.cloned.1.call-start = ((), (), s32[]{:S(2)}) async-start(), calls=%async_computation.7 | async-start | bytes 3145728 | tf_op jit(solution)/shard_map/psum | solution.py:18
  519.3 185.0 %all-to-all-start.3 = ((bf16[384,8,1024]{2,0,1:T(8,128)(2,1)}), bf16[384,8,1024]{2,0,1:T(8,128)(2,1)}, u32[]{:S(2)}, u32[]{:S(2)}) async-start(bf16[384,8,1024]{2,0,1:T(8,128)(2,1)} %bitcast.38), calls=%async_computation.3 | async-start | bytes 12582912 | tf_op jit(solution)/shard_map/all_to_all | solution.py:52
  524.1 136.0 %copy-start.2 = (f32[3072]{0:T(1024)S(1)}, f32[3072]{0:T(1024)}, u32[]{:S(2)}) copy-start(f32[3072]{0:T(1024)} %param.19) | copy-start | bytes 36868
  524.1 180.1 %all-gather.17.cloned.1.call-start = ((), (), s32[]{:S(2)}) async-start(), calls=%async_computation.10 | async-start | bytes 7864320 | tf_op jit(solution)/shard_map/all_gather | solution.py:46
  527.4 273.9 %all-reduce.5.cloned.1.call-start = ((), (), s32[]{:S(2)}) async-start(), calls=%async_computation.11 | async-start | bytes 3145728 | tf_op jit(solution)/shard_map/psum | solution.py:18
  711.9 91.1 %copy-start.3 = (f32[3072]{0:T(1024)S(1)}, f32[3072]{0:T(1024)}, u32[]{:S(2)}) copy-start(f32[3072]{0:T(1024)} %param.21) | copy-start | bytes 36868
  805.6 12.7 %slice-start = ((s8[6291456]{0:T(1024)(128)(4,1)}), s8[4194304]{0:T(1024)(128)(4,1)S(1)}, s32[]{:S(2)}) async-start(s8[6291456]{0:T(1024)(128)(4,1)} %bitcast.34), calls=%async_computation.12 | async-start | bytes 8388608
  812.0 6.4 slice-start.1
  821.0 12.7 %slice-start.2 = ((s8[6291456]{0:T(1024)(128)(4,1)}), s8[4194304]{0:T(1024)(128)(4,1)S(1)}, s32[]{:S(2)}) async-start(s8[6291456]{0:T(1024)(128)(4,1)} %bitcast.36), calls=%async_computation.14 | async-start | bytes 8388608
  827.4 6.4 slice-start.3
Sparse Core Ops, SparseCore 0:
  13.6 49.0 all-gather.6
  64.9 46.3 all-gather.8
  113.4 46.3 all-gather.12
  221.1 46.7 all-gather.14
  364.4 46.6 all-gather.10
  419.0 239.4 all-reduce.2
  660.6 43.5 all-gather.16
  712.1 89.2 all-reduce.4
where the time goes:
time: 844 us; the launch traced here: 843 us
  waiting for transfers between devices  701 us (83%)
  local copies, waits for them, and re-layouts  58.5 us (7%)
  other arithmetic  24.5 us (3%)
  matrix products  24.2 us (3%)
  starting transfers between devices  20.7 us (2%)
  between operations  14.3 us (2%)
    psum x2, waiting for transfers between devices, half_step(): total = lax.psum(partial_value, 'fs')  220 us
    all_to_all x1, waiting for transfers between devices, per_device(): lax.all_to_all(wide[1], 'fs', split_axis=1, concat_axis=0, tiled=True)  131 us
    all_to_all x1, waiting for transfers between devices, per_device(): lax.all_to_all(wide[3], 'fs', split_axis=1, concat_axis=0, tiled=True)  100 us
    all_to_all x1, waiting for transfers between devices, per_device(): lax.all_to_all(wide[0], 'fs', split_axis=1, concat_axis=0, tiled=True)  95.9 us
    all_gather x1, waiting for transfers between devices, per_device(): lax.all_gather((gain_a * gate_first).astype(jnp.bfloat16), 'tp', axis=1,...  48.5 us
    all_gather x1, waiting for transfers between devices, per_device(): lax.all_gather(down_second.astype(jnp.bfloat16), 'tp', axis=1, tiled=True)  38 us
    all_gather x1, waiting for transfers between devices, per_device(): lax.all_gather(down_first.astype(jnp.bfloat16), 'tp', axis=1, tiled=True)  35.5 us
    unnamed x22, local copies, waits for them, and re-layouts  30.9 us
  transfers between devices with their start and end apart: 12, of which 9 were waited for; matrix products, arithmetic and copies ran while one was open for 7% of the time, Pallas kernels for 0%

commit v1 on v0

--- a/solution.py
+++ b/solution.py
@@ -4,6 +4,27 @@
 from jax.sharding import PartitionSpec as P
 
 EPSILON = 1e-06
+
+
+def collect(shard, axis, dim):
+    peers, place, rows = (lax.axis_size(axis), lax.axis_index(axis), shard.shape[dim])
+    ahead = [(i, (i + 1) % peers) for i in range(peers)]
+    behind = [(i, (i - 1) % peers) for i in range(peers)]
+    out = jnp.zeros((*shard.shape[:dim], peers * rows, *shard.shape[dim + 1 :]), shard.dtype)
+    out = lax.dynamic_update_slice_in_dim(out, shard, place * rows, axis=dim)
+    from_left = from_right = shard
+    half = peers // 2
+    for turn in range(1, half + 1):
+        from_left = lax.ppermute(from_left, axis, ahead)
+        out = lax.dynamic_update_slice_in_dim(
+            out, from_left, (place - turn) % peers * rows, axis=dim
+        )
+        if turn < peers - half:
+            from_right = lax.ppermute(from_right, axis, behind)
+            out = lax.dynamic_update_slice_in_dim(
+                out, from_right, (place + turn) % peers * rows, axis=dim
+            )
+    return out
 
 
 def half_step(rows, gate, up, down, post_gain):
@@ -38,7 +59,7 @@
     gain_a = lax.dynamic_slice_in_dim(pre_gain_first, start, height, 0)[:, None]
     gain_b = lax.dynamic_slice_in_dim(pre_gain_second, start, height, 0)[:, None]
     wide = (
-        lax.all_gather((gain_a * gate_first).astype(jnp.bfloat16), "tp", axis=1, tiled=True),
+        collect((gain_a * gate_first).astype(jnp.bfloat16), "tp", 1),
         lax.all_gather((gain_a * up_first).astype(jnp.bfloat16), "tp", axis=1, tiled=True),
         lax.all_gather(down_first.astype(jnp.bfloat16), "tp", axis=1, tiled=True),
         lax.all_gather((gain_b * gate_second).astype(jnp.bfloat16), "tp", axis=1, tiled=True),

time: 844 us -> 878 us (1.040)
  waiting for transfers between devices: 701 us -> 719 us
  starting transfers between devices: 20.7 us -> 30.7 us
    ppermute x0 -> x3, waiting for transfers between devices: none -> 75 us  [the longest x2 75 us: collect(): from_left = lax.ppermute(from_left, axis, ahead)]
    all_gather x1 -> x0, waiting for transfers between devices: 48.5 us -> none  [per_device(): lax.all_gather((gain_a * gate_first).astype(jnp.bfloat16), 'tp', axis=1,...]
    all_to_all x1, waiting for transfers between devices: 95.9 us -> 134 us  [per_device(): lax.all_to_all(wide[0], 'fs', split_axis=1, concat_axis=0, tiled=True)]
    all_gather x1, waiting for transfers between devices: 30.9 us -> 0.02 us  [per_device(): lax.all_gather((gain_a * up_first).astype(jnp.bfloat16), 'tp', axis=1, ti...]
    all_gather x1, waiting for transfers between devices: 35.5 us -> 18.7 us  [per_device(): lax.all_gather(down_first.astype(jnp.bfloat16), 'tp', axis=1, tiled=True)]
    ppermute x0 -> x3, starting transfers between devices: none -> 9.11 us  [the longest x2 7.17 us: collect(): from_left = lax.ppermute(from_left, axis, ahead)]
    unnamed x22 -> x18, local copies, waits for them, and re-layouts: 30.9 us -> 26.1 us
  transfers between devices with their start and end apart: 12 -> 14, of which waited for: 9 -> 9; matrix products, arithmetic and copies ran while one was open for 7% -> 9% of each run, Pallas kernels for 0% -> 0%
where the time goes in v1:
time: 878 us; the launch traced here: 877 us
  waiting for transfers between devices  719 us (82%)
  local copies, waits for them, and re-layouts  66.7 us (8%)
  starting transfers between devices  30.7 us (3%)
  matrix products  23.6 us (3%)
  other arithmetic  22.3 us (3%)
  between operations  14.3 us (2%)
    psum x2, waiting for transfers between devices, half_step(): total = lax.psum(partial_value, 'fs')  220 us
    all_to_all x1, waiting for transfers between devices, per_device(): lax.all_to_all(wide[0], 'fs', split_axis=1, concat_axis=0, tiled=True)  134 us
    all_to_all x1, waiting for transfers between devices, per_device(): lax.all_to_all(wide[1], 'fs', split_axis=1, concat_axis=0, tiled=True)  131 us
    all_to_all x1, waiting for transfers between devices, per_device(): lax.all_to_all(wide[3], 'fs', split_axis=1, concat_axis=0, tiled=True)  101 us
    ppermute x2, waiting for transfers between devices, collect(): from_left = lax.ppermute(from_left, axis, ahead)  75 us
    all_gather x1, waiting for transfers between devices, per_device(): lax.all_gather(down_second.astype(jnp.bfloat16), 'tp', axis=1, tiled=True)  37.7 us
    unnamed x18, local copies, waits for them, and re-layouts  26.1 us
    all_gather x1, waiting for transfers between devices, per_device(): lax.all_gather(down_first.astype(jnp.bfloat16), 'tp', axis=1, tiled=True)  18.7 us
  transfers between devices with their start and end apart: 14, of which 9 were waited for; matrix products, arithmetic and copies ran while one was open for 9% of the time, Pallas kernels for 0%

profile of v1, /device:TPU:0, one launch (start us, length us, event | category | flops | bytes accessed | tf_op | source)
XLA Modules:
  0.0 876.7 jit_solution(7763050995130494224)
XLA Ops:
  7.2 0.0 all-gather.6.cloned.1.call-start
  7.2 2.4 copy.28
  9.6 0.8 dynamic_slice.6
  10.4 1.4 multiply_convert_fusion.2
  11.8 0.0 all-gather.6.cloned.1.call-update
  11.8 2.4 copy.26
  14.2 3.2 broadcast_in_dim.2
  17.4 2.0 constant_dynamic-update-slice_fusion.3
  19.4 0.5 collective-permute-start
  19.9 1.9 collective-permute-start.1
  21.9 61.8 %collective-permute-done = bf16[384,2048]{0,1:T(8,128)(2,1)S(1)} collective-permute-done((bf16[384,2048]{0,1:T(8,128)(2,1)}, bf16[384,2048]{0,1:T(8,128)(2,1)S(1)}, u32[]{:S(2)}, u32[]{:S(2)}) %collective-permute-start) | collective-permute-done | bytes 1572896 | tf_op jit(solution)/shard_map/ppermute | solution.py:18
  83.7 6.7 collective-permute-start.2
  90.4 1.3 constant_dynamic-update-slice_fusion.2
  91.7 2.7 constant_dynamic-update-slice_fusion.1
  94.4 13.2 %collective-permute-done.2 = bf16[384,2048]{0,1:T(8,128)(2,1)S(1)} collective-permute-done((bf16[384,2048]{0,1:T(8,128)(2,1)S(1)}, bf16[384,2048]{0,1:T(8,128)(2,1)S(1)}, u32[]{:S(2)}, u32[]{:S(2)}) %collective-permute-start.2) | collective-permute-done | bytes 1572896 | tf_op jit(solution)/shard_map/ppermute | solution.py:18
  107.6 1.3 constant_dynamic-update-slice_fusion
  108.9 6.8 all-to-all-start
  115.7 0.0 all-gather.10.cloned.1.call-start
  115.8 0.8 dynamic_slice.7
  116.6 4.5 multiply_convert_fusion.1
  121.0 0.0 all-gather.10.cloned.1.call-update
  121.1 0.0 all-gather.6.cloned.1.call-done
  121.1 134.3 %all-to-all-done = bf16[384,8,1024]{0,2,1:T(8,128)(2,1)} async-done(((bf16[384,8,1024]{0,2,1:T(8,128)(2,1)}), bf16[384,8,1024]{0,2,1:T(8,128)(2,1)}, u32[]{:S(2)}, u32[]{:S(2)}) %all-to-all-start) | async-done | bytes 6291488 | tf_op jit(solution)/shard_map/all_to_all | solution.py:70
  255.4 4.8 all-to-all-start.1
  260.2 0.0 all-gather.12.cloned.1.call-start
  260.2 0.7 all-gather.12.cloned.1.call-update
  260.9 0.0 all-gather.10.cloned.1.call-done
  261.0 6.5 copy.37
  267.5 131.3 %all-to-all-done.1 = bf16[384,8,1024]{0,2,1:T(8,128)(2,1)} async-done(((bf16[384,8,1024]{0,2,1:T(8,128)(2,1)}), bf16[384,8,1024]{0,2,1:T(8,128)(2,1)}, u32[]{:S(2)}, u32[]{:S(2)}) %all-to-all-start.1) | async-done | bytes 6291488 | tf_op jit(solution)/shard_map/all_to_all | solution.py:71
  398.7 4.7 all-to-all-start.2
  403.5 0.0 copy-start
  403.5 0.0 all-gather.8.cloned.1.call-start
  403.5 3.2 convert_element_type.47
  406.8 0.0 all-gather.8.cloned.1.call-update
  406.8 0.0 all-reduce.3.cloned.1.call-start
  406.9 0.2 fusion
  407.1 0.0 all-gather.12.cloned.1.call-done
  407.1 6.5 copy.36
  413.6 8.8 %copy.27 = bf16[8,384,1024]{2,1,0:T(8,128)(2,1)} copy(bf16[8,384,1024]{1,2,0:T(8,128)(2,1)} %bitcast.1) | data formatting | bytes 12582912 | tf_op jit(solution)/shard_map/all_to_all | solution.py:70
  422.4 3.9 fusion.26
  426.3 8.6 copy.29
  434.9 18.7 %all-gather.8.cloned.1.call-done = bf16[1024,3072]{1,0:T(8,128)(2,1)} async-done(((bf16[1024,768]{1,0:T(8,128)(2,1)}), bf16[1024,3072]{1,0:T(8,128)(2,1)}) %all-gather.8.cloned.1.call-update) | async-done | bytes 6291472 | tf_op jit(solution)/shard_map/all_gather | solution.py:64
  453.7 7.7 fusion.9
  461.4 0.0 all-reduce.3.cloned.1.call-update
  461.4 100.9 %all-to-all-done.2 = bf16[384,8,1024]{2,0,1:T(8,128)(2,1)} async-done(((bf16[384,8,1024]{2,0,1:T(8,128)(2,1)}), bf16[384,8,1024]{2,0,1:T(8,128)(2,1)}, u32[]{:S(2)}, u32[]{:S(2)}) %all-to-all-start.2) | async-done | bytes 6291488 | tf_op jit(solution)/shard_map/all_to_all | solution.py:72
  562.3 4.8 all-to-all-start.3
  567.1 0.0 all-gather.14.cloned.1.call-start
  567.2 3.2 convert_element_type.54
  570.4 0.0 all-gather.14.cloned.1.call-update
  570.4 0.2 all-reduce.5.cloned.1.call-start
  570.7 130.8 %all-reduce.3.cloned.1.call-done = f32[128,3072]{1,0:T(8,128)} async-done(((f32[128,3072]{1,0:T(8,128)}), f32[128,3072]{1,0:T(8,128)}) %all-reduce.3.cloned.1.call-update) | async-done | bytes 1572880 | tf_op jit(solution)/shard_map/psum | solution.py:39
  701.5 1.6 multiply_reduce_fusion.1
  703.1 1.9 fusion.3
  705.0 4.3 fusion.22
  709.4 37.7 %all-gather.14.cloned.1.call-done = bf16[1024,3072]{1,0:T(8,128)(2,1)} async-done(((bf16[1024,768]{1,0:T(8,128)(2,1)}), bf16[1024,3072]{1,0:T(8,128)(2,1)}) %all-gather.14.cloned.1.call-update) | async-done | bytes 6291472 | tf_op jit(solution)/shard_map/all_gather | solution.py:67
  747.1 7.7 fusion.8
  754.8 0.0 all-reduce.5.cloned.1.call-update
  754.8 89.4 %all-reduce.5.cloned.1.call-done = f32[128,3072]{1,0:T(8,128)} async-done(((f32[128,3072]{1,0:T(8,128)}), f32[128,3072]{1,0:T(8,128)}) %all-reduce.5.cloned.1.call-update) | async-done | bytes 1572880 | tf_op jit(solution)/shard_map/psum | solution.py:39
  844.2 1.6 multiply_reduce_fusion
  845.9 2.6 fusion.5
  848.4 5.9 copy.48
  854.4 6.4 copy.49
  860.8 6.3 copy.50
  867.1 2.7 copy.51
  (18 shorter events, 0.1 us)
Async XLA Ops:
  7.2 113.9 %all-gather.6.cloned.1.call-start = ((), (), s32[]{:S(2)}) async-start(), calls=%async_computation.4 | async-start | bytes 7864320 | tf_op jit(solution)/shard_map/all_gather | solution.py:63
  19.4 64.3 %collective-permute-start = (bf16[384,2048]{0,1:T(8,128)(2,1)}, bf16[384,2048]{0,1:T(8,128)(2,1)S(1)}, u32[]{:S(2)}, u32[]{:S(2)}) collective-permute-start(bf16[384,2048]{0,1:T(8,128)(2,1)} %get-tuple-element.10), channel_id=1, source_target_pairs={{0,1},{1,2},{2,3},{3,0},{4,5},{5,6},{6,7},{7,4},{8,9},{9,10},{10,1... | collective-permute-start | bytes 4718600 | tf_op jit(solution)/shard_map/ppermute | solution.py:18
  19.9 71.8 %collective-permute-start.1 = (bf16[384,2048]{0,1:T(8,128)(2,1)}, bf16[384,2048]{0,1:T(8,128)(2,1)}, u32[]{:S(2)}, u32[]{:S(2)}) collective-permute-start(bf16[384,2048]{0,1:T(8,128)(2,1)} %get-tuple-element.10), channel_id=1, source_target_pairs={{0,3},{1,0},{2,1},{3,2},{4,7},{5,4},{6,5},{7,6},{8,11},{9,8},{10,9... | collective-permute-start | bytes 4718600 | tf_op jit(solution)/shard_map/ppermute | solution.py:23
  83.7 23.9 %collective-permute-start.2 = (bf16[384,2048]{0,1:T(8,128)(2,1)S(1)}, bf16[384,2048]{0,1:T(8,128)(2,1)S(1)}, u32[]{:S(2)}, u32[]{:S(2)}) collective-permute-start(bf16[384,2048]{0,1:T(8,128)(2,1)S(1)} %collective-permute-done), channel_id=1, source_target_pairs={{0,1},{1,2},{2,3},{3,0},{4,5},{5,6},{6,7},{7,4},{8,9},{9,10},{10,1... | collective-permute-start | bytes 4718600 | tf_op jit(solution)/shard_map/ppermute | solution.py:18
  108.9 7.7 copy-start.1
  108.9 146.5 %all-to-all-start = ((bf16[384,8,1024]{0,2,1:T(8,128)(2,1)}), bf16[384,8,1024]{0,2,1:T(8,128)(2,1)}, u32[]{:S(2)}, u32[]{:S(2)}) async-start(bf16[384,8,1024]{0,2,1:T(8,128)(2,1)} %bitcast), calls=%async_computation | async-start | bytes 12582912 | tf_op jit(solution)/shard_map/all_to_all | solution.py:70
  115.7 145.2 %all-gather.10.cloned.1.call-start = ((), (), s32[]{:S(2)}) async-start(), calls=%async_computation.7 | async-start | bytes 7864320 | tf_op jit(solution)/shard_map/all_gather | solution.py:65
  255.4 143.3 %all-to-all-start.1 = ((bf16[384,8,1024]{0,2,1:T(8,128)(2,1)}), bf16[384,8,1024]{0,2,1:T(8,128)(2,1)}, u32[]{:S(2)}, u32[]{:S(2)}) async-start(bf16[384,8,1024]{0,2,1:T(8,128)(2,1)} %bitcast.34), calls=%async_computation.1 | async-start | bytes 12582912 | tf_op jit(solution)/shard_map/all_to_all | solution.py:71
  260.2 146.9 %all-gather.12.cloned.1.call-start = ((), (), s32[]{:S(2)}) async-start(), calls=%async_computation.8 | async-start | bytes 7864320 | tf_op jit(solution)/shard_map/all_gather | solution.py:66
  398.7 163.6 %all-to-all-start.2 = ((bf16[384,8,1024]{2,0,1:T(8,128)(2,1)}), bf16[384,8,1024]{2,0,1:T(8,128)(2,1)}, u32[]{:S(2)}, u32[]{:S(2)}) async-start(bf16[384,8,1024]{2,0,1:T(8,128)(2,1)} %bitcast.31), calls=%async_computation.2 | async-start | bytes 12582912 | tf_op jit(solution)/shard_map/all_to_all | solution.py:72
  403.5 3.4 copy-start
  403.5 50.2 %all-gather.8.cloned.1.call-start = ((), (), s32[]{:S(2)}) async-start(), calls=%async_computation.5 | async-start | bytes 7864320 | tf_op jit(solution)/shard_map/all_gather | solution.py:64
  406.8 294.7 %all-reduce.3.cloned.1.call-start = ((), (), s32[]{:S(2)}) async-start(), calls=%async_computation.6 | async-start | bytes 3145728 | tf_op jit(solution)/shard_map/psum | solution.py:39
  562.3 184.8 %all-to-all-start.3 = ((bf16[384,8,1024]{2,0,1:T(8,128)(2,1)}), bf16[384,8,1024]{2,0,1:T(8,128)(2,1)}, u32[]{:S(2)}, u32[]{:S(2)}) async-start(bf16[384,8,1024]{2,0,1:T(8,128)(2,1)} %bitcast.28), calls=%async_computation.3 | async-start | bytes 12582912 | tf_op jit(solution)/shard_map/all_to_all | solution.py:73
  567.1 136.0 %copy-start.2 = (f32[3072]{0:T(1024)S(1)}, f32[3072]{0:T(1024)}, u32[]{:S(2)}) copy-start(f32[3072]{0:T(1024)} %param.19) | copy-start | bytes 36868
  567.1 180.0 %all-gather.14.cloned.1.call-start = ((), (), s32[]{:S(2)}) async-start(), calls=%async_computation.9 | async-start | bytes 7864320 | tf_op jit(solution)/shard_map/all_gather | solution.py:67
  570.4 273.8 %all-reduce.5.cloned.1.call-start = ((), (), s32[]{:S(2)}) async-start(), calls=%async_computation.10 | async-start | bytes 3145728 | tf_op jit(solution)/shard_map/psum | solution.py:39
  754.8 91.1 %copy-start.3 = (f32[3072]{0:T(1024)S(1)}, f32[3072]{0:T(1024)}, u32[]{:S(2)}) copy-start(f32[3072]{0:T(1024)} %param.21) | copy-start | bytes 36868
  854.4 12.7 %slice-start = ((s8[6291456]{0:T(1024)(128)(4,1)}), s8[4194304]{0:T(1024)(128)(4,1)S(1)}, s32[]{:S(2)}) async-start(s8[6291456]{0:T(1024)(128)(4,1)} %bitcast.29), calls=%async_computation.11 | async-start | bytes 8388608
  860.8 6.4 slice-start.1
Sparse Core Ops, SparseCore 0:
  11.9 81.9 all-gather.5
  121.2 49.6 all-gather.9
  263.1 46.7 all-gather.11
  406.9 46.6 all-gather.7
  461.5 239.9 all-reduce.2
  703.5 43.5 all-gather.13
  754.9 89.2 all-reduce.4
